TPU v7x, 32 devices: a whole 2x2x4 slice. The times are simulated.
32 devices in a mesh: tp: 8 (over z, y), dp: 4 (over x, core).
Axes of the slice: x: 2, y: 2, z: 4, core: 2. Of those that a mesh axis runs over, the one named last changes fastest.
Arguments:
- tokens: bfloat16 [128, 4096], P('tp', 'dp'), may hold values from -10 to 10
- norm_gain: float32 [2, 4096], P(None, 'dp'), may hold values from 0.1 to 1.9
- input_weight: bfloat16 [2, 4096, 1024], P(None, 'dp', 'tp'), may hold values from -0.09375 to 0.09375
- decay_rate: float32 [2, 64, 64], P(None, 'tp'), may hold values from 0.01 to 1
- frequency: float32 [2, 64, 64], P(None, 'tp'), may hold values from 0.5 to 3
- step_size: float32 [2, 64], P(None, 'tp'), may hold values from 0.1 to 1
- state_in: float32 [2, 64, 16, 128], P(None, 'tp'), may hold values from -1.5 to 1.5
- readout: float32 [2, 64, 16, 128], P(None, 'tp'), may hold values from -0.5 to 0.5
- skip_gain: float32 [2, 1024], P(None, 'tp'), may hold values from -3 to 3
- value_weight: bfloat16 [2, 1024, 4096], P(None, 'tp', 'dp'), may hold values from -0.1875 to 0.1875
- gate_weight: bfloat16 [2, 1024, 4096], P(None, 'tp', 'dp'), may hold values from -0.1875 to 0.1875
- states: float32 [2, 128, 64, 128], P(None, 'dp', 'tp'), may hold values from -3 to 3
Outputs:
- tokens_out: bfloat16 [128, 4096], P('tp', 'dp')
- states_out: float32 [2, 128, 64, 128], P(None, 'dp', 'tp')
All inputs are finite; a program needn't handle non-finite values.
Results may differ from a plain program's by a relative error of at most 0.007.
Values may be sent and summed in bfloat16 or wider, within the bound.
No kernel may reach another device: no remote copies, remote signals or barrier semaphores. Data moves between devices by JAX's collectives and lax.ppermute only.
A program may use at most 64 MiB of HBM per device.

v0:
```python
import jax
import jax.numpy as jnp
from jax import lax
from jax.sharding import PartitionSpec as P

D = 4096
LAYERS = 2
epsilon = 1e-06


def transition(rate, frequency, step):
    magnitude = jnp.exp(-rate * step[:, None])
    angle = frequency * step[:, None]
    keep_real = magnitude * jnp.cos(angle)
    keep_imag = magnitude * jnp.sin(angle)
    minus_one = keep_real - 1.0
    denominator = rate * rate + frequency * frequency
    lift_real = (-minus_one * rate + keep_imag * frequency) / denominator
    lift_imag = (-keep_imag * rate - minus_one * frequency) / denominator
    return (keep_real, keep_imag, lift_real, lift_imag)


def update(drive, state, rate, frequency, step, state_in, readout, skip):
    groups = rate.shape[0]
    half = state.shape[-1] // 2
    grouped = drive.reshape(drive.shape[0], groups, -1)
    pushed = jnp.einsum("sgc,gcq->sgq", grouped, state_in, precision=lax.Precision.HIGHEST)
    keep_real, keep_imag, lift_real, lift_imag = transition(rate, frequency, step)
    push_real, push_imag = (pushed[..., :half], pushed[..., half:])
    old_real, old_imag = (state[..., :half], state[..., half:])
    new_real = (
        keep_real * old_real - keep_imag * old_imag + lift_real * push_real - lift_imag * push_imag
    )
    new_imag = (
        keep_real * old_imag + keep_imag * old_real + lift_real * push_imag + lift_imag * push_real
    )
    new_state = jnp.concatenate([new_real, new_imag], axis=-1)
    summed = jnp.einsum("sgq,gcq->sgc", new_state, readout, precision=lax.Precision.HIGHEST)
    value = summed.reshape(drive.shape) + skip[None, :] * drive
    return (new_state, jax.nn.gelu(value).astype(jnp.bfloat16))


def body(
    tokens,
    norm_gain,
    input_weight,
    decay_rate,
    frequency,
    step_size,
    state_in,
    readout,
    skip_gain,
    value_weight,
    gate_weight,
    states,
):
    current = tokens
    own_rows = states.shape[1]
    offset = lax.axis_index("dp") * own_rows
    width_dev = tokens.shape[1]
    updated = []
    for depth_index in range(LAYERS):
        whole = lax.all_gather(current, "tp", axis=0, tiled=True)
        widened = whole.astype(jnp.float32)
        squares = jnp.sum(widened * widened, axis=1)
        gained = (widened * norm_gain[depth_index][None, :]).astype(jnp.bfloat16)
        weight_in = input_weight[depth_index]
        totals = lax.psum(squares, "dp")
        own_squares = lax.dynamic_slice_in_dim(totals, offset, own_rows)
        summed = lax.psum_scatter(
            jnp.dot(gained, weight_in, preferred_element_type=jnp.float32),
            "dp",
            scatter_dimension=0,
            tiled=True,
        )
        drive = summed * lax.rsqrt(own_squares / D + epsilon)[:, None]
        new_state, readout_value = update(
            drive,
            states[depth_index],
            decay_rate[depth_index],
            frequency[depth_index],
            step_size[depth_index],
            state_in[depth_index],
            readout[depth_index],
            skip_gain[depth_index],
        )
        updated.append(new_state)
        ready = lax.all_gather(readout_value, "dp", axis=0, tiled=True)
        value_rows = value_weight[depth_index]
        gate_rows = gate_weight[depth_index]
        both = lax.psum_scatter(
            jnp.concatenate(
                [
                    jnp.dot(ready, value_rows, preferred_element_type=jnp.float32),
                    jnp.dot(ready, gate_rows, preferred_element_type=jnp.float32),
                ],
                axis=1,
            ),
            "tp",
            scatter_dimension=0,
            tiled=True,
        )
        value, gate = (both[:, :width_dev], both[:, width_dev:])
        current = (current.astype(jnp.float32) + value * jax.nn.sigmoid(gate)).astype(jnp.bfloat16)
    return (current, jnp.stack(updated))


def solution(mesh):
    in_specs = (
        P("tp", "dp"),
        P(None, "dp"),
        P(None, "dp", "tp"),
        P(None, "tp", None),
        P(None, "tp", None),
        P(None, "tp"),
        P(None, "tp", None, None),
        P(None, "tp", None, None),
        P(None, "tp"),
        P(None, "tp", "dp"),
        P(None, "tp", "dp"),
        P(None, "dp", "tp", None),
    )
    out_specs = (P("tp", "dp"), P(None, "dp", "tp", None))
    return jax.shard_map(body, mesh=mesh, in_specs=in_specs, out_specs=out_specs, check_vma=False)
```

profile of v0, /device:TPU:0, one launch (start us, length us, event | category | flops | bytes accessed | tf_op | source)
XLA Modules:
  0.0 270.4 jit_solution(15485128415687994219)
XLA Ops:
  7.2 0.0 reduce-scatter.5.cloned.1.call-start
  7.2 0.8 fusion.73
  8.0 32.8 %all_gather.12 = bf16[128,1024]{1,0:T(8,128)(2,1)S(1)} all-gather(bf16[16,1024]{1,0:T(8,128)(2,1)} %param.12), channel_id=1, replica_groups=mesh['tp'=8,'dp'=4] {'tp'}, dimensions={0}, use_global_device_ids=true | all-gather | bytes 294912 | tf_op jit(solution)/shard_map/all_gather | solution.py:63
  40.8 1.8 fusion.6
  42.6 0.0 reduce-scatter.5.cloned.1.call-update
  42.6 0.0 copy-start.11
  42.7 0.0 reduce-scatter.7.cloned.1.call-start
  42.7 0.6 copy-done.10
  43.3 0.0 copy-done.11
  43.4 0.0 copy-start.8
  43.4 0.0 copy-start.9
  43.4 0.1 copy_bitcast_fusion
  43.4 0.6 copy-done.8
  44.1 0.0 copy-done.9
  44.1 0.1 fusion.66
  44.2 0.1 fusion.1
  44.3 5.8 %psum.14 = f32[128]{0:T(128)S(1)} all-reduce(f32[128]{0:T(128)S(1)} %fusion.1), channel_id=1, replica_groups=mesh['tp'=8,'dp'=4] {'dp'}, use_global_device_ids=true, to_apply=%region_2.0 | all-reduce | flops 128 | bytes 1024 | tf_op jit(solution)/shard_map/psum | solution.py:68
  50.1 0.1 add_rsqrt_fusion.1
  50.2 13.1 %reduce-scatter.5.cloned.1.call-done = f32[32,128]{1,0:T(8,128)} async-done(((f32[128,128]{1,0:T(8,128)}), f32[32,128]{1,0:T(8,128)}) %reduce-scatter.5.cloned.1.call-update) | async-done | bytes 16400 | tf_op jit(solution)/shard_map/reduce_scatter | solution.py:70
  63.4 0.8 broadcast_multiply_fusion.1
  64.1 0.1 copy.22
  64.2 0.4 convolution_bitcast_fusion.1
  64.7 0.0 copy-start.5
  64.7 0.0 copy-start
  64.7 0.1 multiply_subtract_fusion.1
  64.8 0.7 copy-done.5
  65.6 0.4 fusion.39
  66.0 0.1 copy.23
  66.0 0.2 copy-done.6
  66.3 0.1 fusion.57
  66.4 5.2 %all_gather.13 = bf16[128,128]{1,0:T(8,128)(2,1)S(1)} all-gather(bf16[32,128]{1,0:T(8,128)(2,1)S(1)} %fusion.57), channel_id=1, replica_groups=mesh['tp'=8,'dp'=4] {'dp'}, dimensions={0}, use_global_device_ids=true | all-gather | bytes 40960 | tf_op jit(solution)/shard_map/all_gather | solution.py:88
  71.6 0.2 fusion.13
  71.8 0.2 fusion.15
  72.0 1.0 pad_maximum_fusion
  73.1 0.0 reduce-scatter.7.cloned.1.call-update
  73.1 0.0 reduce-scatter.9.cloned.1.call-start
  73.1 64.3 %reduce-scatter.7.cloned.1.call-done = f32[16,2048]{1,0:T(8,128)} async-done(((f32[128,2048]{1,0:T(8,128)}), f32[16,2048]{1,0:T(8,128)}) %reduce-scatter.7.cloned.1.call-update) | async-done | bytes 131088 | tf_op jit(solution)/shard_map/reduce_scatter | solution.py:91
  137.4 0.9 fusion.46
  138.3 30.8 %all_gather.14 = bf16[128,1024]{1,0:T(8,128)(2,1)S(1)} all-gather(bf16[16,1024]{1,0:T(8,128)(2,1)S(1)} %fusion.46), channel_id=1, replica_groups=mesh['tp'=8,'dp'=4] {'tp'}, dimensions={0}, use_global_device_ids=true | all-gather | bytes 294912 | tf_op jit(solution)/shard_map/all_gather | solution.py:63
  169.2 0.9 fusion.4
  170.1 0.0 reduce-scatter.9.cloned.1.call-update
  170.1 0.0 reduce-scatter.11.cloned.1.call-start
  170.1 0.1 fusion.3
  170.3 5.7 %psum.15 = f32[128]{0:T(128)S(1)} all-reduce(f32[128]{0:T(128)S(1)} %fusion.3), channel_id=1, replica_groups=mesh['tp'=8,'dp'=4] {'dp'}, use_global_device_ids=true, to_apply=%region_6.0 | all-reduce | flops 128 | bytes 1024 | tf_op jit(solution)/shard_map/psum | solution.py:68
  175.9 0.1 add_rsqrt_fusion
  176.0 12.6 %reduce-scatter.9.cloned.1.call-done = f32[32,128]{1,0:T(8,128)} async-done(((f32[128,128]{1,0:T(8,128)}), f32[32,128]{1,0:T(8,128)}) %reduce-scatter.9.cloned.1.call-update) | async-done | bytes 16400 | tf_op jit(solution)/shard_map/reduce_scatter | solution.py:70
  188.6 0.8 broadcast_multiply_fusion
  189.4 0.1 copy.25
  189.5 0.4 convolution_bitcast_fusion
  190.0 0.1 multiply_subtract_fusion
  190.1 0.4 fusion.36
  190.5 0.1 copy.26
  190.6 0.7 copy-done.7
  191.2 0.1 fusion.65
  191.3 5.2 %all_gather.15 = bf16[128,128]{1,0:T(8,128)(2,1)S(1)} all-gather(bf16[32,128]{1,0:T(8,128)(2,1)S(1)} %fusion.65), channel_id=1, replica_groups=mesh['tp'=8,'dp'=4] {'dp'}, dimensions={0}, use_global_device_ids=true | all-gather | bytes 40960 | tf_op jit(solution)/shard_map/all_gather | solution.py:88
  196.5 0.2 fusion.8
  196.7 0.2 fusion.10
  196.9 1.0 pad_maximum_fusion.1
  198.0 0.0 reduce-scatter.11.cloned.1.call-update
  198.0 0.1 fusion.49
  198.1 0.1 fusion.48
  198.2 0.9 copy.27
  199.1 63.2 %reduce-scatter.11.cloned.1.call-done = f32[16,2048]{1,0:T(8,128)} async-done(((f32[128,2048]{1,0:T(8,128)}), f32[16,2048]{1,0:T(8,128)}) %reduce-scatter.11.cloned.1.call-update) | async-done | bytes 131088 | tf_op jit(solution)/shard_map/reduce_scatter | solution.py:91
  262.4 1.5 fusion.47
  (18 shorter events, 0.1 us)
Async XLA Ops:
  7.2 56.2 %reduce-scatter.5.cloned.1.call-start = ((), (), s32[]{:S(2)}) async-start(), calls=%async_computation.4 | async-start | bytes 81920 | tf_op jit(solution)/shard_map/reduce_scatter | solution.py:70
  40.8 2.6 copy-start.2
  42.6 0.7 copy-start.10
  42.6 0.7 copy-start.11
  42.7 94.8 %reduce-scatter.7.cloned.1.call-start = ((), (), s32[]{:S(2)}) async-start(), calls=%async_computation.5 | async-start | bytes 1179648 | tf_op jit(solution)/shard_map/reduce_scatter | solution.py:91
  43.4 0.7 copy-start.8
  43.4 0.7 copy-start.9
  44.3 19.9 %copy-start.4 = (f32[2,8,16,128]{3,2,1,0:T(8,128)S(1)}, f32[2,8,16,128]{3,2,1,0:T(8,128)}, u32[]{:S(2)}) copy-start(f32[2,8,16,128]{3,2,1,0:T(8,128)} %param.18) | copy-start | bytes 393220
  64.7 0.9 copy-start.5
  64.7 6.9 %copy-start = (bf16[2,128,1024]{2,1,0:T(8,128)(2,1)S(1)}, bf16[2,128,1024]{2,1,0:T(8,128)(2,1)}, u32[]{:S(2)}) copy-start(bf16[2,128,1024]{2,1,0:T(8,128)(2,1)} %param.22) | copy-start | bytes 1572868
  65.6 0.7 copy-start.6
  66.0 5.8 %copy-start.1 = (bf16[2,128,1024]{2,1,0:T(8,128)(2,1)S(1)}, bf16[2,128,1024]{2,1,0:T(8,128)(2,1)}, u32[]{:S(2)}) copy-start(bf16[2,128,1024]{2,1,0:T(8,128)(2,1)} %param.21) | copy-start | bytes 1572868
  73.1 64.4 %copy-start.3 = (bf16[16,1024]{1,0:T(8,128)(2,1)S(1)}, bf16[16,1024]{1,0:T(8,128)(2,1)}, u32[]{:S(2)}) copy-start(bf16[16,1024]{1,0:T(8,128)(2,1)} %param.12) | copy-start | bytes 98308
  73.1 96.1 %copy-start.12 = (bf16[2,1024,128]{2,1,0:T(8,128)(2,1)S(1)}, bf16[2,1024,128]{2,1,0:T(8,128)(2,1)}, u32[]{:S(2)}) copy-start(bf16[2,1024,128]{2,1,0:T(8,128)(2,1)} %param.14) | copy-start | bytes 1572868
  73.1 115.5 %reduce-scatter.9.cloned.1.call-start = ((), (), s32[]{:S(2)}) async-start(), calls=%async_computation.6 | async-start | bytes 81920 | tf_op jit(solution)/shard_map/reduce_scatter | solution.py:70
  170.1 92.3 %reduce-scatter.11.cloned.1.call-start = ((), (), s32[]{:S(2)}) async-start(), calls=%async_computation.7 | async-start | bytes 1179648 | tf_op jit(solution)/shard_map/reduce_scatter | solution.py:91
  190.5 0.7 copy-start.7
Sparse Core Ops, SparseCore 0:
  42.8 20.5 reduce-scatter.4
  73.2 64.1 reduce-scatter.6
  170.2 18.3 reduce-scatter.8
  198.1 64.1 reduce-scatter.10
where the time goes:
time: 271 us; the launch traced here: 270 us
  waiting for transfers between devices  153 us (56%)
  blocking collectives  85.4 us (32%)
  between operations  14 us (5%)
  other arithmetic  7.3 us (3%)
  matrix products  5.18 us (2%)
  local copies, waits for them, and re-layouts  4.96 us (2%)
    reduce_scatter x2, waiting for transfers between devices, body(): lax.psum_scatter(jnp.concatenate([jnp.dot(ready, value_rows, preferred_el...  128 us
    all_gather x2, blocking collectives, body(): whole = lax.all_gather(current, 'tp', axis=0, tiled=True)  63.6 us
    reduce_scatter x2, waiting for transfers between devices, body(): lax.psum_scatter(jnp.dot(gained, weight_in, preferred_element_type=jnp.fl...  25.8 us
    psum x2, blocking collectives, body(): totals = lax.psum(squares, 'dp')  11.5 us
    all_gather x2, blocking collectives, body(): ready = lax.all_gather(readout_value, 'dp', axis=0, tiled=True)  10.4 us
  transfers between devices with their start and end apart: 4, of which 4 were waited for; matrix products, arithmetic and copies ran while one was open for 1% of the time, Pallas kernels for 0%

commit v1 on v0

--- a/solution.py
+++ b/solution.py
@@ -6,6 +6,17 @@
 D = 4096
 LAYERS = 2
 epsilon = 1e-06
+
+
+def turned_line(x, axis, along):
+    size = lax.axis_size(axis)
+    right = [(i, (i + 1) % size) for i in range(size)]
+    blocks = [x]
+    for reach in range(1, size):
+        blocks = [lax.ppermute(blocks[0], axis, right), *blocks]
+    whole = jnp.concatenate(blocks, axis=along)
+    offset = (lax.axis_index(axis) + 1) * blocks[-1].shape[along]
+    return jnp.roll(whole, offset, axis=along)
 
 
 def transition(rate, frequency, step):
@@ -60,7 +71,7 @@
     width_dev = tokens.shape[1]
     updated = []
     for depth_index in range(LAYERS):
-        whole = lax.all_gather(current, "tp", axis=0, tiled=True)
+        whole = turned_line(current, "tp", 0)
         widened = whole.astype(jnp.float32)
         squares = jnp.sum(widened * widened, axis=1)
         gained = (widened * norm_gain[depth_index][None, :]).astype(jnp.bfloat16)

time: 271 us -> 296 us (1.092)
  waiting for transfers between devices: 153 us -> 239 us
  blocking collectives: 85.4 us -> 21.7 us
  starting transfers between devices: 0.16 us -> 4.35 us
    ppermute x0 -> x14, waiting for transfers between devices: none -> 89.2 us  [turned_line(): blocks = [lax.ppermute(blocks[0], axis, right), *blocks]]
    all_gather x2 -> x0, blocking collectives: 63.6 us -> none  [body(): whole = lax.all_gather(current, 'tp', axis=0, tiled=True)]
    ppermute x0 -> x14, starting transfers between devices: none -> 4.19 us  [turned_line(): blocks = [lax.ppermute(blocks[0], axis, right), *blocks]]
    reduce_scatter x2, waiting for transfers between devices: 25.8 us -> 21.9 us  [body(): lax.psum_scatter(jnp.dot(gained, weight_in, preferred_element_type=jnp.fl...]
  transfers between devices with their start and end apart: 4 -> 18, of which waited for: 4 -> 18; matrix products, arithmetic and copies ran while one was open for 1% -> 1% of each run, Pallas kernels for 0% -> 0%
where the time goes in v1:
time: 296 us; the launch traced here: 295 us
  waiting for transfers between devices  239 us (81%)
  blocking collectives  21.7 us (7%)
  between operations  14.1 us (5%)
  other arithmetic  7.55 us (3%)
  local copies, waits for them, and re-layouts  4.72 us (2%)
  starting transfers between devices  4.35 us (1%)
  matrix products  4.32 us (1%)
    reduce_scatter x2, waiting for transfers between devices, body(): lax.psum_scatter(jnp.concatenate([jnp.dot(ready, value_rows, preferred_el...  128 us
    ppermute x14, waiting for transfers between devices, turned_line(): blocks = [lax.ppermute(blocks[0], axis, right), *blocks]  89.2 us
    reduce_scatter x2, waiting for transfers between devices, body(): lax.psum_scatter(jnp.dot(gained, weight_in, preferred_element_type=jnp.fl...  21.9 us
    psum x2, blocking collectives, body(): totals = lax.psum(squares, 'dp')  11.3 us
    all_gather x2, blocking collectives, body(): ready = lax.all_gather(readout_value, 'dp', axis=0, tiled=True)  10.4 us
  transfers between devices with their start and end apart: 18, of which 18 were waited for; matrix products, arithmetic and copies ran while one was open for 1% of the time, Pallas kernels for 0%

profile of v1, /device:TPU:0, one launch (start us, length us, event | category | flops | bytes accessed | tf_op | source)
XLA Modules:
  0.0 295.5 jit_solution(9293903349074095734)
XLA Ops:
  7.2 3.0 %collective-permute-start = (bf16[16,1024]{1,0:T(8,128)(2,1)}, bf16[16,1024]{1,0:T(8,128)(2,1)S(1)}, u32[]{:S(2)}, u32[]{:S(2)}) collective-permute-start(bf16[16,1024]{1,0:T(8,128)(2,1)} %param.14), channel_id=1, source_target_pairs={{0,4},{4,8},{8,12},{12,16},{16,20},{20,24},{24,28},{28,0},{1,5},{5... | collective-permute-start | bytes 98312 | tf_op jit(solution)/shard_map/ppermute | solution.py:16
  10.3 5.1 %collective-permute-done = bf16[16,1024]{1,0:T(8,128)(2,1)S(1)} collective-permute-done((bf16[16,1024]{1,0:T(8,128)(2,1)}, bf16[16,1024]{1,0:T(8,128)(2,1)S(1)}, u32[]{:S(2)}, u32[]{:S(2)}) %collective-permute-start) | collective-permute-done | bytes 32800 | tf_op jit(solution)/shard_map/ppermute | solution.py:16
  15.4 1.0 fusion.76
  16.4 5.6 %collective-permute-done.1 = bf16[16,1024]{1,0:T(8,128)(2,1)S(1)} collective-permute-done((bf16[16,1024]{1,0:T(8,128)(2,1)S(1)}, bf16[16,1024]{1,0:T(8,128)(2,1)S(1)}, u32[]{:S(2)}, u32[]{:S(2)}) %collective-permute-start.1) | collective-permute-done | bytes 32800 | tf_op jit(solution)/shard_map/ppermute | solution.py:16
  22.0 0.1 copy_bitcast_fusion
  22.1 6.5 %collective-permute-done.2 = bf16[16,1024]{1,0:T(8,128)(2,1)S(1)} collective-permute-done((bf16[16,1024]{1,0:T(8,128)(2,1)S(1)}, bf16[16,1024]{1,0:T(8,128)(2,1)S(1)}, u32[]{:S(2)}, u32[]{:S(2)}) %collective-permute-start.2) | collective-permute-done | bytes 32800 | tf_op jit(solution)/shard_map/ppermute | solution.py:16
  28.6 6.6 %collective-permute-done.3 = bf16[16,1024]{1,0:T(8,128)(2,1)S(1)} collective-permute-done((bf16[16,1024]{1,0:T(8,128)(2,1)S(1)}, bf16[16,1024]{1,0:T(8,128)(2,1)S(1)}, u32[]{:S(2)}, u32[]{:S(2)}) %collective-permute-start.3) | collective-permute-done | bytes 32800 | tf_op jit(solution)/shard_map/ppermute | solution.py:16
  35.3 0.1 fusion.68
  35.4 6.8 %collective-permute-done.4 = bf16[16,1024]{1,0:T(8,128)(2,1)S(1)} collective-permute-done((bf16[16,1024]{1,0:T(8,128)(2,1)S(1)}, bf16[16,1024]{1,0:T(8,128)(2,1)S(1)}, u32[]{:S(2)}, u32[]{:S(2)}) %collective-permute-start.4) | collective-permute-done | bytes 32800 | tf_op jit(solution)/shard_map/ppermute | solution.py:16
  42.2 6.6 %collective-permute-done.5 = bf16[16,1024]{1,0:T(8,128)(2,1)S(1)} collective-permute-done((bf16[16,1024]{1,0:T(8,128)(2,1)S(1)}, bf16[16,1024]{1,0:T(8,128)(2,1)S(1)}, u32[]{:S(2)}, u32[]{:S(2)}) %collective-permute-start.5) | collective-permute-done | bytes 32800 | tf_op jit(solution)/shard_map/ppermute | solution.py:16
  48.8 6.6 %collective-permute-done.6 = bf16[16,1024]{1,0:T(8,128)(2,1)S(1)} collective-permute-done((bf16[16,1024]{1,0:T(8,128)(2,1)S(1)}, bf16[16,1024]{1,0:T(8,128)(2,1)S(1)}, u32[]{:S(2)}, u32[]{:S(2)}) %collective-permute-start.6) | collective-permute-done | bytes 32800 | tf_op jit(solution)/shard_map/ppermute | solution.py:16
  55.5 0.7 copy-done.2
  56.2 0.9 fusion.8
  57.2 0.0 reduce-scatter.7.cloned.1.call-start
  57.2 0.2 fusion.1
  57.5 5.7 %psum.14 = f32[128]{0:T(128)S(1)} all-reduce(f32[128]{0:T(128)S(1)} %fusion.1), channel_id=1, replica_groups=mesh['tp'=8,'dp'=4] {'dp'}, use_global_device_ids=true, to_apply=%region_2.4 | all-reduce | flops 128 | bytes 1024 | tf_op jit(solution)/shard_map/psum | solution.py:79
  63.1 0.1 add_rsqrt_fusion.1
  63.2 11.0 %reduce-scatter.5.cloned.1.call-done = f32[32,128]{1,0:T(8,128)} async-done(((f32[128,128]{1,0:T(8,128)}), f32[32,128]{1,0:T(8,128)}) %reduce-scatter.5.cloned.1.call-update) | async-done | bytes 16400 | tf_op jit(solution)/shard_map/reduce_scatter | solution.py:81
  74.2 0.8 broadcast_multiply_fusion.1
  75.0 0.1 copy.22
  75.1 0.4 convolution_bitcast_fusion.1
  75.5 0.1 multiply_subtract_fusion.1
  75.7 0.7 copy-done.4
  76.4 0.4 fusion.41
  76.8 0.1 copy.23
  76.9 0.2 copy-done.6
  77.1 0.1 fusion.59
  77.2 5.2 %all_gather.6 = bf16[128,128]{1,0:T(8,128)(2,1)S(1)} all-gather(bf16[32,128]{1,0:T(8,128)(2,1)S(1)} %fusion.59), channel_id=1, replica_groups=mesh['tp'=8,'dp'=4] {'dp'}, dimensions={0}, use_global_device_ids=true | all-gather | bytes 40960 | tf_op jit(solution)/shard_map/all_gather | solution.py:99
  82.4 0.2 fusion.15
  82.6 0.2 fusion.17
  82.8 1.1 pad_maximum_fusion
  84.0 64.4 %reduce-scatter.7.cloned.1.call-done = f32[16,2048]{1,0:T(8,128)} async-done(((f32[128,2048]{1,0:T(8,128)}), f32[16,2048]{1,0:T(8,128)}) %reduce-scatter.7.cloned.1.call-update) | async-done | bytes 131088 | tf_op jit(solution)/shard_map/reduce_scatter | solution.py:102
  148.3 0.9 fusion.48
  149.2 1.1 collective-permute-start.7
  150.4 5.6 %collective-permute-done.7 = bf16[16,1024]{1,0:T(8,128)(2,1)S(1)} collective-permute-done((bf16[16,1024]{1,0:T(8,128)(2,1)S(1)}, bf16[16,1024]{1,0:T(8,128)(2,1)S(1)}, u32[]{:S(2)}, u32[]{:S(2)}) %collective-permute-start.7) | collective-permute-done | bytes 32800 | tf_op jit(solution)/shard_map/ppermute | solution.py:16
  155.9 6.6 %collective-permute-done.8 = bf16[16,1024]{1,0:T(8,128)(2,1)S(1)} collective-permute-done((bf16[16,1024]{1,0:T(8,128)(2,1)S(1)}, bf16[16,1024]{1,0:T(8,128)(2,1)S(1)}, u32[]{:S(2)}, u32[]{:S(2)}) %collective-permute-start.8) | collective-permute-done | bytes 32800 | tf_op jit(solution)/shard_map/ppermute | solution.py:16
  162.5 6.7 %collective-permute-done.9 = bf16[16,1024]{1,0:T(8,128)(2,1)S(1)} collective-permute-done((bf16[16,1024]{1,0:T(8,128)(2,1)S(1)}, bf16[16,1024]{1,0:T(8,128)(2,1)S(1)}, u32[]{:S(2)}, u32[]{:S(2)}) %collective-permute-start.9) | collective-permute-done | bytes 32800 | tf_op jit(solution)/shard_map/ppermute | solution.py:16
  169.2 6.6 %collective-permute-done.10 = bf16[16,1024]{1,0:T(8,128)(2,1)S(1)} collective-permute-done((bf16[16,1024]{1,0:T(8,128)(2,1)S(1)}, bf16[16,1024]{1,0:T(8,128)(2,1)S(1)}, u32[]{:S(2)}, u32[]{:S(2)}) %collective-permute-start.10) | collective-permute-done | bytes 32800 | tf_op jit(solution)/shard_map/ppermute | solution.py:16
  175.9 6.6 %collective-permute-done.11 = bf16[16,1024]{1,0:T(8,128)(2,1)S(1)} collective-permute-done((bf16[16,1024]{1,0:T(8,128)(2,1)S(1)}, bf16[16,1024]{1,0:T(8,128)(2,1)S(1)}, u32[]{:S(2)}, u32[]{:S(2)}) %collective-permute-start.11) | collective-permute-done | bytes 32800 | tf_op jit(solution)/shard_map/ppermute | solution.py:16
  182.5 6.6 %collective-permute-done.12 = bf16[16,1024]{1,0:T(8,128)(2,1)S(1)} collective-permute-done((bf16[16,1024]{1,0:T(8,128)(2,1)S(1)}, bf16[16,1024]{1,0:T(8,128)(2,1)S(1)}, u32[]{:S(2)}, u32[]{:S(2)}) %collective-permute-start.12) | collective-permute-done | bytes 32800 | tf_op jit(solution)/shard_map/ppermute | solution.py:16
  189.1 6.6 %collective-permute-done.13 = bf16[16,1024]{1,0:T(8,128)(2,1)S(1)} collective-permute-done((bf16[16,1024]{1,0:T(8,128)(2,1)S(1)}, bf16[16,1024]{1,0:T(8,128)(2,1)S(1)}, u32[]{:S(2)}, u32[]{:S(2)}) %collective-permute-start.13) | collective-permute-done | bytes 32800 | tf_op jit(solution)/shard_map/ppermute | solution.py:16
  195.8 0.9 fusion.6
  196.7 0.0 reduce-scatter.11.cloned.1.call-start
  196.8 0.2 fusion.3
  197.0 5.7 %psum.15 = f32[128]{0:T(128)S(1)} all-reduce(f32[128]{0:T(128)S(1)} %fusion.3), channel_id=1, replica_groups=mesh['tp'=8,'dp'=4] {'dp'}, use_global_device_ids=true, to_apply=%region_6.8 | all-reduce | flops 128 | bytes 1024 | tf_op jit(solution)/shard_map/psum | solution.py:79
  202.7 0.1 add_rsqrt_fusion
  202.7 10.9 %reduce-scatter.9.cloned.1.call-done = f32[32,128]{1,0:T(8,128)} async-done(((f32[128,128]{1,0:T(8,128)}), f32[32,128]{1,0:T(8,128)}) %reduce-scatter.9.cloned.1.call-update) | async-done | bytes 16400 | tf_op jit(solution)/shard_map/reduce_scatter | solution.py:81
  213.7 0.8 broadcast_multiply_fusion
  214.4 0.1 copy.25
  214.5 0.4 convolution_bitcast_fusion
  215.0 0.1 multiply_subtract_fusion
  215.1 0.4 fusion.38
  215.5 0.1 copy.26
  215.6 0.7 copy-done.5
  216.2 0.1 fusion.67
  216.3 5.2 %all_gather.7 = bf16[128,128]{1,0:T(8,128)(2,1)S(1)} all-gather(bf16[32,128]{1,0:T(8,128)(2,1)S(1)} %fusion.67), channel_id=1, replica_groups=mesh['tp'=8,'dp'=4] {'dp'}, dimensions={0}, use_global_device_ids=true | all-gather | bytes 40960 | tf_op jit(solution)/shard_map/all_gather | solution.py:99
  221.5 0.2 fusion.10
  221.7 0.2 fusion.12
  222.0 1.1 pad_maximum_fusion.1
  223.1 0.1 fusion.51
  223.2 0.1 fusion.50
  223.3 0.9 copy.27
  224.2 63.3 %reduce-scatter.11.cloned.1.call-done = f32[16,2048]{1,0:T(8,128)} async-done(((f32[128,2048]{1,0:T(8,128)}), f32[16,2048]{1,0:T(8,128)}) %reduce-scatter.11.cloned.1.call-update) | async-done | bytes 131088 | tf_op jit(solution)/shard_map/reduce_scatter | solution.py:102
  287.4 1.5 fusion.49
  (60 shorter events, 0.3 us)
Async XLA Ops:
  7.2 67.0 %reduce-scatter.5.cloned.1.call-start = ((), (), s32[]{:S(2)}) async-start(), calls=%async_computation.4 | async-start | bytes 81920 | tf_op jit(solution)/shard_map/reduce_scatter | solution.py:81
  7.2 8.2 %collective-permute-start = (bf16[16,1024]{1,0:T(8,128)(2,1)}, bf16[16,1024]{1,0:T(8,128)(2,1)S(1)}, u32[]{:S(2)}, u32[]{:S(2)}) collective-permute-start(bf16[16,1024]{1,0:T(8,128)(2,1)} %param.14), channel_id=1, source_target_pairs={{0,4},{4,8},{8,12},{12,16},{16,20},{20,24},{24,28},{28,0},{1,5},{5... | collective-permute-start | bytes 98312 | tf_op jit(solution)/shard_map/ppermute | solution.py:16
  15.4 6.6 %collective-permute-start.1 = (bf16[16,1024]{1,0:T(8,128)(2,1)S(1)}, bf16[16,1024]{1,0:T(8,128)(2,1)S(1)}, u32[]{:S(2)}, u32[]{:S(2)}) collective-permute-start(bf16[16,1024]{1,0:T(8,128)(2,1)S(1)} %collective-permute-done), channel_id=1, source_target_pairs={{0,4},{4,8},{8,12},{12,16},{16,20},{20,24},{24,28},{28,0},{1,5},{5... | collective-permute-start | bytes 98312 | tf_op jit(solution)/shard_map/ppermute | solution.py:16
  22.0 6.6 %collective-permute-start.2 = (bf16[16,1024]{1,0:T(8,128)(2,1)S(1)}, bf16[16,1024]{1,0:T(8,128)(2,1)S(1)}, u32[]{:S(2)}, u32[]{:S(2)}) collective-permute-start(bf16[16,1024]{1,0:T(8,128)(2,1)S(1)} %collective-permute-done.1), channel_id=1, source_target_pairs={{0,4},{4,8},{8,12},{12,16},{16,20},{20,24},{24,28},{28,0},{1,5},{5... | collective-permute-start | bytes 98312 | tf_op jit(solution)/shard_map/ppermute | solution.py:16
  22.0 6.6 %copy-start.10 = (f32[2,8]{1,0:T(2,128)S(1)}, f32[2,8]{1,0:T(2,128)}, u32[]{:S(2)}) copy-start(f32[2,8]{1,0:T(2,128)} %param.19) | copy-start | bytes 196
  22.0 13.2 %copy-start.7 = (f32[2,8,64]{2,1,0:T(8,128)S(1)}, f32[2,8,64]{2,1,0:T(8,128)}, u32[]{:S(2)}) copy-start(f32[2,8,64]{2,1,0:T(8,128)} %param.18) | copy-start | bytes 12292
  22.0 13.2 %copy-start.8 = (f32[2,8,64]{2,1,0:T(8,128)S(1)}, f32[2,8,64]{2,1,0:T(8,128)}, u32[]{:S(2)}) copy-start(f32[2,8,64]{2,1,0:T(8,128)} %param.17) | copy-start | bytes 12292
  22.0 34.2 %copy-start.12 = (bf16[2,1024,128]{2,1,0:T(8,128)(2,1)S(1)}, bf16[2,1024,128]{2,1,0:T(8,128)(2,1)}, u32[]{:S(2)}) copy-start(bf16[2,1024,128]{2,1,0:T(8,128)(2,1)} %param.16) | copy-start | bytes 1572868
  28.6 6.6 %collective-permute-start.3 = (bf16[16,1024]{1,0:T(8,128)(2,1)S(1)}, bf16[16,1024]{1,0:T(8,128)(2,1)S(1)}, u32[]{:S(2)}, u32[]{:S(2)}) collective-permute-start(bf16[16,1024]{1,0:T(8,128)(2,1)S(1)} %collective-permute-done.2), channel_id=1, source_target_pairs={{0,4},{4,8},{8,12},{12,16},{16,20},{20,24},{24,28},{28,0},{1,5},{5... | collective-permute-start | bytes 98312 | tf_op jit(solution)/shard_map/ppermute | solution.py:16
  35.2 7.0 %collective-permute-start.4 = (bf16[16,1024]{1,0:T(8,128)(2,1)S(1)}, bf16[16,1024]{1,0:T(8,128)(2,1)S(1)}, u32[]{:S(2)}, u32[]{:S(2)}) collective-permute-start(bf16[16,1024]{1,0:T(8,128)(2,1)S(1)} %collective-permute-done.3), channel_id=1, source_target_pairs={{0,4},{4,8},{8,12},{12,16},{16,20},{20,24},{24,28},{28,0},{1,5},{5... | collective-permute-start | bytes 98312 | tf_op jit(solution)/shard_map/ppermute | solution.py:16
  35.2 6.9 %copy-start.9 = (f32[2,1024]{1,0:T(2,128)S(1)}, f32[2,1024]{1,0:T(2,128)}, u32[]{:S(2)}) copy-start(f32[2,1024]{1,0:T(2,128)} %param.15) | copy-start | bytes 24580
  35.4 13.4 %copy-start.11 = (f32[2,128]{1,0:T(2,128)S(1)}, f32[2,128]{1,0:T(2,128)}, u32[]{:S(2)}) copy-start(f32[2,128]{1,0:T(2,128)} %param.22) | copy-start | bytes 3076
  42.2 6.6 %collective-permute-start.5 = (bf16[16,1024]{1,0:T(8,128)(2,1)S(1)}, bf16[16,1024]{1,0:T(8,128)(2,1)S(1)}, u32[]{:S(2)}, u32[]{:S(2)}) collective-permute-start(bf16[16,1024]{1,0:T(8,128)(2,1)S(1)} %collective-permute-done.4), channel_id=1, source_target_pairs={{0,4},{4,8},{8,12},{12,16},{16,20},{20,24},{24,28},{28,0},{1,5},{5... | collective-permute-start | bytes 98312 | tf_op jit(solution)/shard_map/ppermute | solution.py:16
  48.8 6.6 %collective-permute-start.6 = (bf16[16,1024]{1,0:T(8,128)(2,1)S(1)}, bf16[16,1024]{1,0:T(8,128)(2,1)S(1)}, u32[]{:S(2)}, u32[]{:S(2)}) collective-permute-start(bf16[16,1024]{1,0:T(8,128)(2,1)S(1)} %collective-permute-done.5), channel_id=1, source_target_pairs={{0,4},{4,8},{8,12},{12,16},{16,20},{20,24},{24,28},{28,0},{1,5},{5... | collective-permute-start | bytes 98312 | tf_op jit(solution)/shard_map/ppermute | solution.py:16
  55.5 0.8 copy-start.2
  57.2 17.9 %copy-start.3 = (f32[2,8,16,128]{3,2,1,0:T(8,128)S(1)}, f32[2,8,16,128]{3,2,1,0:T(8,128)}, u32[]{:S(2)}) copy-start(f32[2,8,16,128]{3,2,1,0:T(8,128)} %param.20) | copy-start | bytes 393220
  57.2 91.1 %reduce-scatter.7.cloned.1.call-start = ((), (), s32[]{:S(2)}) async-start(), calls=%async_computation.5 | async-start | bytes 1179648 | tf_op jit(solution)/shard_map/reduce_scatter | solution.py:102
  75.5 0.9 copy-start.4
  75.5 6.9 %copy-start = (bf16[2,128,1024]{2,1,0:T(8,128)(2,1)S(1)}, bf16[2,128,1024]{2,1,0:T(8,128)(2,1)}, u32[]{:S(2)}) copy-start(bf16[2,128,1024]{2,1,0:T(8,128)(2,1)} %param.24) | copy-start | bytes 1572868
  76.4 0.7 copy-start.6
  76.8 5.8 %copy-start.1 = (bf16[2,128,1024]{2,1,0:T(8,128)(2,1)S(1)}, bf16[2,128,1024]{2,1,0:T(8,128)(2,1)}, u32[]{:S(2)}) copy-start(bf16[2,128,1024]{2,1,0:T(8,128)(2,1)} %param.23) | copy-start | bytes 1572868
  83.9 129.7 %reduce-scatter.9.cloned.1.call-start = ((), (), s32[]{:S(2)}) async-start(), calls=%async_computation.6 | async-start | bytes 81920 | tf_op jit(solution)/shard_map/reduce_scatter | solution.py:81
  149.2 6.7 %collective-permute-start.7 = (bf16[16,1024]{1,0:T(8,128)(2,1)S(1)}, bf16[16,1024]{1,0:T(8,128)(2,1)S(1)}, u32[]{:S(2)}, u32[]{:S(2)}) collective-permute-start(bf16[16,1024]{1,0:T(8,128)(2,1)S(1)} %fusion.48), channel_id=1, source_target_pairs={{0,4},{4,8},{8,12},{12,16},{16,20},{20,24},{24,28},{28,0},{1,5},{5... | collective-permute-start | bytes 98312 | tf_op jit(solution)/shard_map/ppermute | solution.py:16
  155.9 6.6 %collective-permute-start.8 = (bf16[16,1024]{1,0:T(8,128)(2,1)S(1)}, bf16[16,1024]{1,0:T(8,128)(2,1)S(1)}, u32[]{:S(2)}, u32[]{:S(2)}) collective-permute-start(bf16[16,1024]{1,0:T(8,128)(2,1)S(1)} %collective-permute-done.7), channel_id=1, source_target_pairs={{0,4},{4,8},{8,12},{12,16},{16,20},{20,24},{24,28},{28,0},{1,5},{5... | collective-permute-start | bytes 98312 | tf_op jit(solution)/shard_map/ppermute | solution.py:16
  162.5 6.7 %collective-permute-start.9 = (bf16[16,1024]{1,0:T(8,128)(2,1)S(1)}, bf16[16,1024]{1,0:T(8,128)(2,1)S(1)}, u32[]{:S(2)}, u32[]{:S(2)}) collective-permute-start(bf16[16,1024]{1,0:T(8,128)(2,1)S(1)} %collective-permute-done.8), channel_id=1, source_target_pairs={{0,4},{4,8},{8,12},{12,16},{16,20},{20,24},{24,28},{28,0},{1,5},{5... | collective-permute-start | bytes 98312 | tf_op jit(solution)/shard_map/ppermute | solution.py:16
  169.2 6.6 %collective-permute-start.10 = (bf16[16,1024]{1,0:T(8,128)(2,1)S(1)}, bf16[16,1024]{1,0:T(8,128)(2,1)S(1)}, u32[]{:S(2)}, u32[]{:S(2)}) collective-permute-start(bf16[16,1024]{1,0:T(8,128)(2,1)S(1)} %collective-permute-done.9), channel_id=1, source_target_pairs={{0,4},{4,8},{8,12},{12,16},{16,20},{20,24},{24,28},{28,0},{1,5},{5... | collective-permute-start | bytes 98312 | tf_op jit(solution)/shard_map/ppermute | solution.py:16
  175.9 6.6 %collective-permute-start.11 = (bf16[16,1024]{1,0:T(8,128)(2,1)S(1)}, bf16[16,1024]{1,0:T(8,128)(2,1)S(1)}, u32[]{:S(2)}, u32[]{:S(2)}) collective-permute-start(bf16[16,1024]{1,0:T(8,128)(2,1)S(1)} %collective-permute-done.10), channel_id=1, source_target_pairs={{0,4},{4,8},{8,12},{12,16},{16,20},{20,24},{24,28},{28,0},{1,5},{5... | collective-permute-start | bytes 98312 | tf_op jit(solution)/shard_map/ppermute | solution.py:16
  182.5 6.6 %collective-permute-start.12 = (bf16[16,1024]{1,0:T(8,128)(2,1)S(1)}, bf16[16,1024]{1,0:T(8,128)(2,1)S(1)}, u32[]{:S(2)}, u32[]{:S(2)}) collective-permute-start(bf16[16,1024]{1,0:T(8,128)(2,1)S(1)} %collective-permute-done.11), channel_id=1, source_target_pairs={{0,4},{4,8},{8,12},{12,16},{16,20},{20,24},{24,28},{28,0},{1,5},{5... | collective-permute-start | bytes 98312 | tf_op jit(solution)/shard_map/ppermute | solution.py:16
  189.1 6.6 %collective-permute-start.13 = (bf16[16,1024]{1,0:T(8,128)(2,1)S(1)}, bf16[16,1024]{1,0:T(8,128)(2,1)S(1)}, u32[]{:S(2)}, u32[]{:S(2)}) collective-permute-start(bf16[16,1024]{1,0:T(8,128)(2,1)S(1)} %collective-permute-done.12), channel_id=1, source_target_pairs={{0,4},{4,8},{8,12},{12,16},{16,20},{20,24},{24,28},{28,0},{1,5},{5... | collective-permute-start | bytes 98312 | tf_op jit(solution)/shard_map/ppermute | solution.py:16
  196.7 90.7 %reduce-scatter.11.cloned.1.call-start = ((), (), s32[]{:S(2)}) async-start(), calls=%async_computation.7 | async-start | bytes 1179648 | tf_op jit(solution)/shard_map/reduce_scatter | solution.py:102
  215.5 0.7 copy-start.5
Sparse Core Ops, SparseCore 0:
  57.3 16.8 reduce-scatter.4
  84.1 64.2 reduce-scatter.6
  196.8 16.7 reduce-scatter.8
  223.2 64.2 reduce-scatter.10
